TPU v7x, 32 devices: a whole 2x2x4 slice. The times are simulated.
32 devices in a mesh: ep: 8 (over z, y), tp: 4 (over x, core).
Axes of the slice: x: 2, y: 2, z: 4, core: 2. Of those that a mesh axis runs over, the one named last changes fastest.
Arguments:
- queries: bfloat16 [8192, 1024], P('ep', 'tp'), may hold values from -6 to 6
- key_rows: bfloat16 [8192, 256], P('ep', 'tp'), may hold values from -6 to 6
- values: bfloat16 [8192, 256], P('ep', 'tp'), may hold values from -6 to 6
- sink_logit: float32 [16], P('tp'), may hold values from 3 to 7
- out_weight: bfloat16 [1024, 2048], P('tp'), may hold values from -0.1875 to 0.1875
- out_gain: float32 [2048], replicated, may hold values from 0.1 to 1.9
- routed_tokens: bfloat16 [16384, 2048], P(('ep', 'tp')), may hold values from -6 to 6
- expert_ids: int32 [16384, 2], P(('ep', 'tp')), may hold values from 0 to 31, as said below
- route_weight: float32 [16384, 2], P(('ep', 'tp')), may hold values from 0.1 to 1
- routed_gain: float32 [2048], replicated, may hold values from 0.1 to 1.9
- expert_gate: bfloat16 [32, 2048, 1024], P('ep', None, 'tp'), may hold values from -0.125 to 0.125
- expert_up: bfloat16 [32, 2048, 1024], P('ep', None, 'tp'), may hold values from -0.125 to 0.125
- expert_down: bfloat16 [32, 2048, 1024], P('ep', None, 'tp'), may hold values from -0.1875 to 0.1875
Outputs:
- mixer_out: bfloat16 [8192, 2048], P(('ep', 'tp'))
- experts_out: bfloat16 [16384, 2048], P(('ep', 'tp'))
Inputs may be any that keep to these rules, and one draw needn't show every extreme that they name: `expert_ids`: both experts of a row lie in one group (equal id // 8); the 512 rows of one device name every group exactly 512 / 4 times; the rows of one device name no expert more than 64 times; in every device's rows some expert of each group is named exactly 64 times, and one expert is named exactly 64 times by the rows of every device.
All inputs are finite; a program needn't handle non-finite values.
Results may differ from a plain program's by a relative error of at most 0.0071.
Values may be sent and summed in bfloat16 or wider, within the bound.
A program may use at most 192 MiB of HBM per device.

v0:
```python
import jax
import jax.numpy as jnp
from jax import lax
from jax.sharding import PartitionSpec as P

HEAD_DIM = 64
WINDOW = 128
QBLOCK = 512
EXPERTS = 32
TOP = 2
CAP = 64


epsilon = 1e-06


def padded(block, sides, width):
    for axis, dim in sides:
        count = lax.axis_size(axis)
        forward = [(i, i + 1) for i in range(count - 1)]
        backward = [(target, source) for source, target in forward]
        low = lax.ppermute(
            lax.slice_in_dim(block, block.shape[dim] - width, None, axis=dim), axis, forward
        )
        high = lax.ppermute(lax.slice_in_dim(block, 0, width, axis=dim), axis, backward)
        block = jnp.concatenate([low, block, high], axis=dim)
    return block


def local(
    queries,
    key_rows,
    values,
    sink_logit,
    out_weight,
    out_gain,
    routed_tokens,
    expert_ids,
    route_weight,
    routed_gain,
    expert_gate,
    expert_up,
    expert_down,
):
    row_count = queries.shape[0]
    heads_here = queries.shape[1] // HEAD_DIM
    kv_here = key_rows.shape[1] // HEAD_DIM
    group_size = heads_here // kv_here
    width = out_weight.shape[1]
    paired = jnp.concatenate((key_rows, values), axis=1)
    extended = padded(paired, (("ep", 0),), WINDOW)
    offset = lax.axis_index("ep") * row_count
    seq_total = row_count * lax.axis_size("ep")
    grouped = queries.reshape(row_count, kv_here, group_size, HEAD_DIM)
    sinks = sink_logit.reshape(kv_here, group_size)[:, :, None, None]
    span_keys = QBLOCK + 2 * WINDOW

    def attend_block(block_index):
        start_row = block_index * QBLOCK
        query_block = lax.dynamic_slice_in_dim(grouped, start_row, QBLOCK, 0)
        band = lax.dynamic_slice_in_dim(extended, start_row, span_keys, 0)
        key_block = band[:, : kv_here * HEAD_DIM].reshape(span_keys, kv_here, HEAD_DIM)
        value_block = band[:, kv_here * HEAD_DIM :].reshape(span_keys, kv_here, HEAD_DIM)
        scores = jnp.einsum(
            "qhgd,khd->hgqk", query_block, key_block, preferred_element_type=jnp.float32
        ) * HEAD_DIM ** (-0.5)
        query_pos = offset + start_row + jnp.arange(QBLOCK, dtype=jnp.int32)
        key_pos = offset + start_row - WINDOW + jnp.arange(span_keys, dtype=jnp.int32)
        valid = (
            (jnp.abs(key_pos[None, :] - query_pos[:, None]) <= WINDOW)
            & (key_pos[None, :] >= 0)
            & (key_pos[None, :] < seq_total)
        )
        masked = jnp.where(valid, scores, -1e30)
        largest = jnp.maximum(jnp.max(masked, axis=-1, keepdims=True), sinks)
        raised = jnp.where(valid, jnp.exp(masked - largest), 0.0)
        denominator = jnp.sum(raised, axis=-1, keepdims=True) + jnp.exp(sinks - largest)
        weights = (raised / denominator).astype(jnp.bfloat16)
        attended = jnp.einsum(
            "hgqk,khd->qhgd", weights, value_block, preferred_element_type=jnp.float32
        )
        return attended.astype(jnp.bfloat16).reshape(QBLOCK, heads_here * HEAD_DIM)

    attended = lax.map(attend_block, jnp.arange(row_count // QBLOCK, dtype=jnp.int32))
    attended = attended.reshape(row_count, heads_here * HEAD_DIM)
    mixed = lax.psum_scatter(
        jnp.dot(attended, out_weight, preferred_element_type=jnp.float32),
        "tp",
        scatter_dimension=0,
        tiled=True,
    )
    mixer_out = (
        mixed * lax.rsqrt(jnp.mean(mixed * mixed, axis=-1, keepdims=True) + epsilon) * out_gain
    ).astype(jnp.bfloat16)
    token_total = routed_tokens.shape[0]
    inputs = routed_tokens.astype(jnp.float32)
    normed = (
        inputs
        * lax.rsqrt(jnp.mean(inputs * inputs, axis=-1, keepdims=True) + epsilon)
        * routed_gain
    ).astype(jnp.bfloat16)
    flat_ids = expert_ids.reshape(-1)
    onehot = (flat_ids[:, None] == jnp.arange(EXPERTS, dtype=jnp.int32)[None, :]).astype(jnp.int32)
    earlier = jnp.cumsum(onehot, axis=0) - onehot
    slot_index = jnp.sum(earlier * onehot, axis=1)
    flat_dest = slot_index * EXPERTS + flat_ids
    source_rows = jnp.arange(token_total * TOP, dtype=jnp.int32) // TOP
    slot_token = jnp.full((CAP * EXPERTS,), token_total, jnp.int32).at[flat_dest].set(source_rows)
    outgoing = jnp.take(normed, slot_token, axis=0, mode="fill", fill_value=0).reshape(
        1, CAP, EXPERTS, width
    )
    arrived = lax.all_to_all(outgoing, "ep", split_axis=2, concat_axis=0, tiled=True)
    source_count, slot_count, local_experts, feature_count = arrived.shape
    rows_in = arrived.reshape(source_count * slot_count, local_experts, feature_count)
    gate_piece = lax.all_gather(expert_gate, "tp", axis=2, tiled=True)
    up_piece = lax.all_gather(expert_up, "tp", axis=2, tiled=True)
    down_piece = lax.all_gather(expert_down, "tp", axis=2, tiled=True)
    gate = jnp.einsum("red,edf->ref", rows_in, gate_piece, preferred_element_type=jnp.float32)
    upward = jnp.einsum("red,edf->ref", rows_in, up_piece, preferred_element_type=jnp.float32)
    hidden = (jax.nn.silu(gate) * upward).astype(jnp.bfloat16)
    summed = jnp.einsum("ref,edf->red", hidden, down_piece, preferred_element_type=jnp.float32)
    produced = summed.astype(jnp.bfloat16).reshape(
        source_count, slot_count, local_experts, feature_count
    )
    returned = lax.all_to_all(produced, "ep", split_axis=0, concat_axis=2, tiled=True)
    returned = returned.reshape(CAP * EXPERTS, width)
    picked_rows = jnp.take(returned, flat_dest, axis=0).reshape(token_total, TOP, width)
    experts_out = jnp.sum(
        picked_rows.astype(jnp.float32) * route_weight[:, :, None], axis=1
    ).astype(jnp.bfloat16)
    return (mixer_out, experts_out)


def solution(mesh):
    placed = (
        P("ep", "tp"),
        P("ep", "tp"),
        P("ep", "tp"),
        P("tp"),
        P("tp", None),
        P(),
        P(("ep", "tp"), None),
        P(("ep", "tp"), None),
        P(("ep", "tp"), None),
        P(),
        P("ep", None, "tp"),
        P("ep", None, "tp"),
        P("ep", None, "tp"),
    )
    return jax.shard_map(
        local,
        mesh=mesh,
        in_specs=placed,
        out_specs=(P(("ep", "tp"), None), P(("ep", "tp"), None)),
        check_vma=False,
    )
```

profile of v0, /device:TPU:0, one launch (start us, length us, event | category | flops | bytes accessed | tf_op | source)
XLA Modules:
  0.0 638.6 jit_solution(18265312052773669787)
XLA Ops:
  10.1 9.0 %reduce-window.6 = s32[32,8,128]{2,1,0:T(8,128)S(1)} reduce-window(s32[32,8,128]{2,1,0:T(8,128)S(1)} %fusion.28, s32[]{:T(128)} %constant.129.clone.1), window={size=1x1x128 pad=0_0x0_0x127_0}, to_apply=%region_6.7 | reduce-window | flops 4161536 | bytes 262148 | tf_op jit(solution)/shard_map/reduce-window
  20.3 4.3 scatter_custom_fusion
  27.9 11.0 %gather_fusion = bf16[2048,2048]{1,0:T(8,128)(2,1)} fusion(bf16[512,2048]{1,0:T(8,128)(2,1)S(1)} %fusion.24, s32[2048]{0:T(1024)S(1)} %fusion.29), kind=kCustom, calls=%fused_computation | custom fusion | bytes 16785408 | tf_op jit(solution)/shard_map/jit(_take)/gather | solution.py:109
  39.0 16.8 %copy_select_fusion = bf16[1,64,32,2048]{3,1,0,2:T(8,128)(2,1)} fusion(bf16[1,64,32,2048]{3,2,1,0:T(8,128)(2,1)} %bitcast.124, pred[64,32]{0,1:T(8,128)(4,1)S(1)} %copy.59), kind=kLoop, calls=%fused_computation.37 | loop fusion | flops 4194304 | bytes 16779264 | tf_op jit(solution)/shard_map/jit(_take)/select_n | solution.py:109
  55.7 7.2 %all-to-all-start = ((bf16[1,64,32,2048]{3,1,0,2:T(8,128)(2,1)}), bf16[1,64,32,2048]{3,1,0,2:T(8,128)(2,1)}, u32[]{:S(2)}, u32[]{:S(2)}) async-start(bf16[1,64,32,2048]{3,1,0,2:T(8,128)(2,1)} %copy_select_fusion), calls=%async_computation.1 | async-start | bytes 16777216 | tf_op jit(solution)/shard_map/all_to_all | solution.py:112
  69.7 62.0 %collective-permute-done = bf16[128,128]{0,1:T(8,128)(2,1)S(1)} collective-permute-done((bf16[128,128]{0,1:T(8,128)(2,1)S(1)}, bf16[128,128]{0,1:T(8,128)(2,1)S(1)}, u32[]{:S(2)}, u32[]{:S(2)}) %collective-permute-start) | collective-permute-done | bytes 32800 | tf_op jit(solution)/shard_map/ppermute | solution.py:22
  131.8 26.2 %while.12 = (s32[]{:T(128)}, bf16[2,512,256]{2,1,0:T(8,128)(2,1)S(1)}, s32[2]{0:T(128)S(1)}, bf16[1280,128]{0,1:T(8,128)(2,1)S(1)}, s32[]{:T(128)}, /*index=5*/b...) while((s32[]{:T(128)}, ...), condition=%wide.region_3.4_spmd, body=%wide.region_0.3_spmd.sunk | while | flops 426778112 | bytes 47478104 | solution.py:84
  140.0 5.0 fusion.57
  152.8 5.0 fusion.57
  158.1 4.5 fusion.37
  162.6 83.9 %all-to-all-done = bf16[1,64,32,2048]{3,1,0,2:T(8,128)(2,1)} async-done(((bf16[1,64,32,2048]{3,1,0,2:T(8,128)(2,1)}), bf16[1,64,32,2048]{3,1,0,2:T(8,128)(2,1)}, u32[]{:S(2)}, u32[]{:S(2)}) %all-to-all-start) | async-done | bytes 8388640 | tf_op jit(solution)/shard_map/all_to_all | solution.py:112
  246.5 8.9 %copy.61 = bf16[8,1,64,4,2048]{4,2,0,3,1:T(8,128)(2,1)} copy(bf16[8,1,64,4,2048]{4,2,3,0,1:T(8,128)(2,1)} %bitcast.20) | data formatting | bytes 16777216 | tf_op jit(solution)/shard_map/all_to_all | solution.py:112
  255.4 17.1 %fusion.38 = f32[4,512,1024]{2,1,0:T(8,128)} fusion(bf16[512,4,2048]{2,0,1:T(8,128)(2,1)} %bitcast.125, bf16[4,2048,1024]{2,1,0:T(8,128)(2,1)} %all-gather.6.cloned.1.call-done), kind=kOutput, calls=%fused_computation.81 | convolution fusion | flops 8589934592 | bytes 33554432 | tf_op jit(solution)/shard_map/red,edf->ref/dot_general | solution.py:119
  272.5 67.5 %all-gather.8.cloned.1.call-done = bf16[4,2048,1024]{2,1,0:T(8,128)(2,1)} async-done(((bf16[4,2048,256]{2,1,0:T(8,128)(2,1)}), bf16[4,2048,1024]{2,1,0:T(8,128)(2,1)}) %all-gather.8.cloned.1.call-update) | async-done | bytes 16777232 | tf_op jit(solution)/shard_map/all_gather | solution.py:117
  340.0 28.9 %convolution_convert_fusion = bf16[4,512,2048]{2,1,0:T(8,128)(2,1)} fusion(bf16[4,2048,1024]{2,1,0:T(8,128)(2,1)} %all-gather.8.cloned.1.call-done, f32[4,512,1024]{2,1,0:T(8,128)} %fusion.38, bf16[512,4,2048]{2,0,1:T(8,128)(2,1)} %bitcast.126, bf16[4,2048,1024]{2,1,0:T(8,128)(2,1)} %all-gather.4.cloned.1.call-done), kind=kOutput, calls=%fused_computation.40 | convolution fusion | flops 17196646400 | bytes 58720256 | tf_op jit(solution)/shard_map/ref,edf->red/dot_general | solution.py:121
  368.9 8.3 %copy.62 = bf16[8,64,4,2048]{3,1,2,0:T(8,128)(2,1)} copy(bf16[8,64,4,2048]{3,1,0,2:T(8,128)(2,1)} %bitcast.127) | data formatting | bytes 16777216 | tf_op jit(solution)/shard_map/reshape | solution.py:122
  377.2 5.7 all-to-all-start.1
  383.6 30.2 %reduce-scatter.2.cloned.1.call-done = f32[256,2048]{1,0:T(8,128)} async-done(((f32[1024,2048]{1,0:T(8,128)}), f32[256,2048]{1,0:T(8,128)}) %reduce-scatter.2.cloned.1.call-update) | async-done | bytes 2097168 | tf_op jit(solution)/shard_map/reduce_scatter | solution.py:86
  418.5 147.9 %all-to-all-done.1 = bf16[8,64,4,2048]{3,1,2,0:T(8,128)(2,1)} async-done(((bf16[8,64,4,2048]{3,1,2,0:T(8,128)(2,1)}), bf16[8,64,4,2048]{3,1,2,0:T(8,128)(2,1)}, u32[]{:S(2)}, u32[]{:S(2)}) %all-to-all-start.1) | async-done | bytes 8388640 | tf_op jit(solution)/shard_map/all_to_all | solution.py:125
  566.4 12.1 %copy.63 = bf16[1,64,8,4,2048]{4,3,2,1,0:T(4,128)(2,1)} copy(bf16[1,64,8,4,2048]{4,1,3,2,0:T(8,128)(2,1)} %bitcast.27) | data formatting | bytes 16777216 | tf_op jit(solution)/shard_map/all_to_all | solution.py:125
  578.5 12.5 %reshape.271 = bf16[2048,2048]{1,0:T(8,128)(2,1)} reshape(bf16[1,64,8,4,2048]{4,3,2,1,0:T(4,128)(2,1)} %copy.63) | data formatting | bytes 16777216 | tf_op jit(solution)/shard_map/reshape | solution.py:126
  591.0 13.4 %gather_fusion.1 = bf16[1024,2048]{1,0:T(8,128)(2,1)} fusion(bf16[2048,2048]{1,0:T(8,128)(2,1)} %reshape.271, s32[1024]{0:T(1024)S(1)} %broadcast_clamp_fusion), kind=kCustom, calls=%fused_computation.1 | custom fusion | bytes 8392704 | tf_op jit(solution)/shard_map/jit(_take)/gather | solution.py:127
  604.4 7.6 %gather.15 = bf16[512,2,2048]{2,1,0:T(2,128)(2,1)} reshape(bf16[1024,2048]{1,0:T(8,128)(2,1)} %gather_fusion.1) | data formatting | bytes 8388608 | tf_op jit(solution)/shard_map/jit(_take)/gather | solution.py:127
  612.0 20.0 %multiply_reduce_fusion = bf16[512,2048]{1,0:T(8,128)(2,1)} fusion(bf16[512,2,2048]{2,1,0:T(2,128)(2,1)} %gather.15, pred[512,2]{1,0:T(8,128)(4,1)S(1)} %copy.57, f32[512,2]{1,0:T(8,128)S(1)} %copy.64), kind=kLoop, calls=%fused_computation.38 | loop fusion | flops 7340032 | bytes 6296576 | tf_op jit(solution)/shard_map/reduce_sum | solution.py:128
  (107 shorter events, 34.0 us)
Async XLA Ops:
  7.2 150.9 %copy-start = (bf16[256,2048]{1,0:T(8,128)(2,1)S(1)}, bf16[256,2048]{1,0:T(8,128)(2,1)}, u32[]{:S(2)}) copy-start(bf16[256,2048]{1,0:T(8,128)(2,1)} %param.19) | copy-start | bytes 3145732
  7.2 2.3 copy-start.9
  7.2 248.2 %all-gather.6.cloned.1.call-start = ((), (), s32[]{:S(2)}) async-start(), calls=%async_computation.5 | async-start | bytes 20971520 | tf_op jit(solution)/shard_map/all_gather | solution.py:116
  7.9 16.9 %copy-start.3 = (bf16[512,2048]{1,0:T(8,128)(2,1)S(1)}, bf16[512,2048]{1,0:T(8,128)(2,1)}, u32[]{:S(2)}) copy-start(bf16[512,2048]{1,0:T(8,128)(2,1)} %param.21) | copy-start | bytes 6291460
  7.9 17.4 %copy-start.13 = (f32[2048]{0:T(1024)S(1)}, f32[2048]{0:T(1024)}, u32[]{:S(2)}) copy-start(f32[2048]{0:T(1024)} %param.24) | copy-start | bytes 24580
  7.9 264.5 %all-gather.4.cloned.1.call-start = ((), (), s32[]{:S(2)}) async-start(), calls=%async_computation.4 | async-start | bytes 20971520 | tf_op jit(solution)/shard_map/all_gather | solution.py:115
  8.7 331.3 %all-gather.8.cloned.1.call-start = ((), (), s32[]{:S(2)}) async-start(), calls=%async_computation.6 | async-start | bytes 20971520 | tf_op jit(solution)/shard_map/all_gather | solution.py:117
  20.3 4.3 copy-start.11
  55.7 7.3 %copy-start.4 = (bf16[1024,64]{0,1:T(8,128)(2,1)S(1)}, bf16[1024,64]{0,1:T(8,128)(2,1)}, u32[]{:S(2)}) copy-start(bf16[1024,64]{0,1:T(8,128)(2,1)} %param.16) | copy-start | bytes 393220
  55.7 7.3 %copy-start.5 = (bf16[1024,64]{0,1:T(8,128)(2,1)S(1)}, bf16[1024,64]{0,1:T(8,128)(2,1)}, u32[]{:S(2)}) copy-start(bf16[1024,64]{0,1:T(8,128)(2,1)} %param.17) | copy-start | bytes 393220
  55.7 76.1 %copy-start.6 = (f32[4]{0:T(128)S(1)}, f32[4]{0:T(128)}, u32[]{:S(2)}) copy-start(f32[4]{0:T(128)} %param.18) | copy-start | bytes 52
  55.7 190.7 %all-to-all-start = ((bf16[1,64,32,2048]{3,1,0,2:T(8,128)(2,1)}), bf16[1,64,32,2048]{3,1,0,2:T(8,128)(2,1)}, u32[]{:S(2)}, u32[]{:S(2)}) async-start(bf16[1,64,32,2048]{3,1,0,2:T(8,128)(2,1)} %copy_select_fusion), calls=%async_computation.1 | async-start | bytes 16777216 | tf_op jit(solution)/shard_map/all_to_all | solution.py:112
  63.0 350.9 %reduce-scatter.2.cloned.1.call-start = ((), (), s32[]{:S(2)}) async-start(), calls=%async_computation.3 | async-start | bytes 10485760 | tf_op jit(solution)/shard_map/reduce_scatter | solution.py:86
  63.1 68.7 %collective-permute-start = (bf16[128,128]{0,1:T(8,128)(2,1)S(1)}, bf16[128,128]{0,1:T(8,128)(2,1)S(1)}, u32[]{:S(2)}, u32[]{:S(2)}) collective-permute-start(bf16[128,128]{0,1:T(8,128)(2,1)S(1)} %get-tuple-element.110), channel_id=1, source_target_pairs={{0,4},{4,8},{8,12},{12,16},{16,20},{20,24},{24,28},{1,5},{5,9},{9,... | collective-permute-start | bytes 98312 | tf_op jit(solution)/shard_map/ppermute | solution.py:22
  67.0 64.8 %collective-permute-start.1 = (bf16[128,128]{0,1:T(8,128)(2,1)S(1)}, bf16[128,128]{0,1:T(8,128)(2,1)S(1)}, u32[]{:S(2)}, u32[]{:S(2)}) collective-permute-start(bf16[128,128]{0,1:T(8,128)(2,1)S(1)} %get-tuple-element.111), channel_id=1, source_target_pairs={{4,0},{8,4},{12,8},{16,12},{20,16},{24,20},{28,24},{5,1},{9,5},{13... | collective-permute-start | bytes 98312 | tf_op jit(solution)/shard_map/ppermute | solution.py:25
  135.1 3.2 copy-start.2
  148.5 2.7 copy-start.2
  377.1 5.8 copy-start.8
  377.1 6.1 copy-start.10
  377.1 6.3 copy-start.15
  377.1 6.5 %copy-start.12 = (s32[1024,1]{0,1:T(1,128)S(1)}, s32[1024,1]{0,1:T(1,128)}, u32[]{:S(2)}) copy-start(s32[1024,1]{0,1:T(1,128)} %copy-done.11) | copy-start | bytes 12292
  377.1 38.5 %copy-start.14 = (f32[2048]{0:T(1024)S(1)}, f32[2048]{0:T(1024)}, u32[]{:S(2)}) copy-start(f32[2048]{0:T(1024)} %param.20) | copy-start | bytes 24580
  377.2 189.2 %all-to-all-start.1 = ((bf16[8,64,4,2048]{3,1,2,0:T(8,128)(2,1)}), bf16[8,64,4,2048]{3,1,2,0:T(8,128)(2,1)}, u32[]{:S(2)}, u32[]{:S(2)}) async-start(bf16[8,64,4,2048]{3,1,2,0:T(8,128)(2,1)} %copy.62), calls=%async_computation.2 | async-start | bytes 16777216 | tf_op jit(solution)/shard_map/all_to_all | solution.py:125
  591.0 41.0 %copy-start.1 = (bf16[256,2048]{1,0:T(8,128)(2,1)S(1)}, bf16[256,2048]{1,0:T(8,128)(2,1)}, u32[]{:S(2)}) copy-start(bf16[256,2048]{1,0:T(8,128)(2,1)} %param.19) | copy-start | bytes 3145732
  (1 other events, 0.6 us)
Sparse Core Ops, SparseCore 0:
  9.5 110.8 all-gather.5
  122.0 108.1 all-gather.3
  231.8 108.1 all-gather.7
  342.4 71.4 reduce-scatter.1
where the time goes:
time: 640 us; the launch traced here: 639 us
  waiting for transfers between devices  394 us (62%)
  local copies, waits for them, and re-layouts  89 us (14%)
  matrix products  63 us (10%)
  other arithmetic  58.9 us (9%)
  starting transfers between devices  18.5 us (3%)
  between operations  14.1 us (2%)
    all_to_all x1, waiting for transfers between devices, local(): lax.all_to_all(produced, 'ep', split_axis=0, concat_axis=2, tiled=True)  148 us
    all_to_all x1, waiting for transfers between devices, local(): lax.all_to_all(outgoing, 'ep', split_axis=2, concat_axis=0, tiled=True)  83.9 us
    all_gather x1, waiting for transfers between devices, local(): down_piece = lax.all_gather(expert_down, 'tp', axis=2, tiled=True)  67.5 us
    ppermute x1, waiting for transfers between devices, padded(): lax.ppermute(lax.slice_in_dim(block, block.shape[dim] - width, None, axis...  62 us
    reduce_scatter x1, waiting for transfers between devices, local(): lax.psum_scatter(jnp.dot(attended, out_weight, preferred_element_type=jnp...  30.2 us
    dot_general x1, matrix products, local(): jnp.einsum('ref,edf->red', hidden, down_piece, preferred_element_type=jnp...  28.9 us
    gather x2, local copies, waits for them, and re-layouts, local(): jnp.take(returned, flat_dest, axis=0).reshape(token_total, TOP, width)  21 us
    reduce_sum x1, other arithmetic, local(): jnp.sum(picked_rows.astype(jnp.float32) * route_weight[:, :, None], axis=1)  20 us
  transfers between devices with their start and end apart: 8, of which 5 were waited for; matrix products, arithmetic and copies ran while one was open for 22% of the time, Pallas kernels for 0%

commit v1 on v0

v1 whole, which is shorter than its diff:
```python
import functools

import jax
import jax.numpy as jnp
from jax import lax
from jax.experimental import pallas as pl
from jax.experimental.pallas import tpu as pltpu
from jax.sharding import Mesh, PartitionSpec as P

HEAD_DIM = 64
WINDOW = 128
QBLOCK = 512
EXPERTS = 32
EPG = 8
TOP = 2
GROUPS = EXPERTS // EPG
CHUNK_ROWS = 2048
ROW_TILE = 512

epsilon = 1e-06
EP = ("group", "member")
PLANE = ("member", "tp")


def padded(block, width):
    count = lax.axis_size(EP)
    forward = [(i, i + 1) for i in range(count - 1)]
    backward = [(target, source) for source, target in forward]
    low = lax.ppermute(block[-width:], EP, forward)
    high = lax.ppermute(block[:width], EP, backward)
    return jnp.concatenate([low, block, high], axis=0)


def attention(queries, key_rows, values, sink_logit, out_weight, out_gain):
    row_count = queries.shape[0]
    heads_here = queries.shape[1] // HEAD_DIM
    kv_here = key_rows.shape[1] // HEAD_DIM
    group_size = heads_here // kv_here
    full_weight = lax.all_gather(out_weight, "tp", axis=0, tiled=True)
    paired = jnp.concatenate((key_rows, values), axis=1)
    extended = padded(paired, WINDOW)
    offset = lax.axis_index(EP) * row_count
    seq_total = row_count * lax.axis_size(EP)
    grouped = queries.reshape(row_count, kv_here, group_size, HEAD_DIM)
    sinks = sink_logit.reshape(kv_here, group_size)[:, :, None, None]
    span_keys = QBLOCK + 2 * WINDOW

    def attend_block(block_index):
        start_row = block_index * QBLOCK
        query_block = lax.dynamic_slice_in_dim(grouped, start_row, QBLOCK, 0)
        band = lax.dynamic_slice_in_dim(extended, start_row, span_keys, 0)
        key_block = band[:, : kv_here * HEAD_DIM].reshape(span_keys, kv_here, HEAD_DIM)
        value_block = band[:, kv_here * HEAD_DIM :].reshape(span_keys, kv_here, HEAD_DIM)
        scores = jnp.einsum(
            "qhgd,khd->hgqk", query_block, key_block, preferred_element_type=jnp.float32
        ) * HEAD_DIM ** (-0.5)
        query_pos = offset + start_row + jnp.arange(QBLOCK, dtype=jnp.int32)
        key_pos = offset + start_row - WINDOW + jnp.arange(span_keys, dtype=jnp.int32)
        valid = (
            (jnp.abs(key_pos[None, :] - query_pos[:, None]) <= WINDOW)
            & (key_pos[None, :] >= 0)
            & (key_pos[None, :] < seq_total)
        )
        masked = jnp.where(valid, scores, -1e30)
        largest = jnp.maximum(jnp.max(masked, axis=-1, keepdims=True), sinks)
        raised = jnp.where(valid, jnp.exp(masked - largest), 0.0)
        denominator = jnp.sum(raised, axis=-1, keepdims=True) + jnp.exp(sinks - largest)
        weights = (raised / denominator).astype(jnp.bfloat16)
        attended = jnp.einsum(
            "hgqk,khd->qhgd", weights, value_block, preferred_element_type=jnp.float32
        )
        return attended.astype(jnp.bfloat16).reshape(QBLOCK, heads_here * HEAD_DIM)

    attended = lax.map(attend_block, jnp.arange(row_count // QBLOCK, dtype=jnp.int32))
    attended = attended.reshape(row_count, heads_here * HEAD_DIM)
    attended = lax.all_to_all(attended, "tp", split_axis=0, concat_axis=1, tiled=True)
    mixed = jnp.dot(attended, full_weight, preferred_element_type=jnp.float32)
    return (
        mixed * lax.rsqrt(jnp.mean(mixed * mixed, axis=-1, keepdims=True) + epsilon) * out_gain
    ).astype(jnp.bfloat16)


def expert_kernel(x_ref, w_ref, gate_ref, up_ref, down_ref, out_ref, total):
    x = x_ref[...]
    for e in range(gate_ref.shape[0]):
        gate = jnp.dot(x, gate_ref[e], preferred_element_type=jnp.float32)
        upward = jnp.dot(x, up_ref[e], preferred_element_type=jnp.float32)
        hidden = (gate / (1.0 + jnp.exp(-gate)) * upward * w_ref[:, e : e + 1]).astype(
            jnp.bfloat16
        )
        part = lax.dot_general(
            hidden, down_ref[e], (((1,), (1,)), ((), ())), preferred_element_type=jnp.float32
        )
        if e == 0:
            total[...] = part
        else:
            total[...] += part
    out_ref[...] = total[...].astype(jnp.bfloat16)


def apply_experts(rows, weights, gate, up, down):
    count, width = rows.shape
    local_experts, _, units = gate.shape
    tile = min(ROW_TILE, count)
    whole = lambda i: (0, 0, 0)
    return pl.pallas_call(
        expert_kernel,
        grid=(count // tile,),
        out_shape=jax.ShapeDtypeStruct((count, width), jnp.bfloat16),
        in_specs=[
            pl.BlockSpec((tile, width), lambda i: (i, 0)),
            pl.BlockSpec((tile, local_experts), lambda i: (i, 0)),
            pl.BlockSpec(gate.shape, whole, pipeline_mode=pl.Buffered(1)),
            pl.BlockSpec(up.shape, whole, pipeline_mode=pl.Buffered(1)),
            pl.BlockSpec(down.shape, whole, pipeline_mode=pl.Buffered(1)),
        ],
        out_specs=pl.BlockSpec((tile, width), lambda i: (i, 0)),
        scratch_shapes=[pltpu.VMEM((tile, width), jnp.float32)],
        compiler_params=pltpu.CompilerParams(vmem_limit_bytes=48 * 2**20),
        cost_estimate=pl.CostEstimate(
            flops=6 * count * width * local_experts * units,
            bytes_accessed=4 * count * width + 6 * local_experts * units * width,
            transcendentals=count * local_experts * units,
        ),
    )(rows, weights, gate, up, down)


def routed(tokens, expert_ids, route_weight, gain, gate, up, down):
    token_total, width = tokens.shape
    share = token_total // GROUPS
    plane = lax.axis_size(PLANE)
    local_experts = gate.shape[0]
    inputs = tokens.astype(jnp.float32)
    normed = (
        inputs * lax.rsqrt(jnp.mean(inputs * inputs, axis=-1, keepdims=True) + epsilon) * gain
    ).astype(jnp.bfloat16)
    group = expert_ids[:, 0] // EPG
    in_group = (group[:, None] == jnp.arange(GROUPS, dtype=jnp.int32)).astype(jnp.float32)
    index = jnp.arange(token_total, dtype=jnp.int32)
    before = (index[None, :] < index[:, None]).astype(jnp.float32)
    ranks = jnp.dot(before, in_group, preferred_element_type=jnp.float32)
    rank = jnp.sum(ranks * in_group, axis=1).astype(jnp.int32)
    position = group * share + rank
    order = (position[None, :] == index[:, None]).astype(jnp.bfloat16)
    back = (position[:, None] == index[None, :]).astype(jnp.bfloat16)
    ordered = jnp.dot(order, normed, preferred_element_type=jnp.float32).astype(jnp.bfloat16)
    member = jnp.arange(EPG, dtype=jnp.int32)
    spread = jnp.sum(
        jnp.where((expert_ids % EPG)[:, :, None] == member, route_weight[:, :, None], 0.0), axis=1
    )
    spread = jnp.dot(
        order.astype(jnp.float32), spread, precision=lax.Precision.HIGHEST,
        preferred_element_type=jnp.float32,
    )
    spread = spread.reshape(GROUPS, share, EPG).transpose(0, 2, 1).reshape(GROUPS, EPG * share)
    spread = lax.all_to_all(spread, "group", 0, 0, tiled=True)
    spread = lax.all_gather(spread, PLANE, axis=0, tiled=True)
    spread = spread.reshape(plane, GROUPS, EPG, share)
    mine = lax.dynamic_slice_in_dim(
        spread, lax.axis_index("member") * local_experts, local_experts, 2
    ).transpose(0, 1, 3, 2)
    piece = max(min(share, CHUNK_ROWS // (plane * GROUPS)), 16)
    ordered = ordered.reshape(GROUPS, share, width)
    results = []
    for start in range(0, share, piece):
        sent = lax.all_to_all(ordered[:, start : start + piece], "group", 0, 0, tiled=True)
        sent = sent.reshape(GROUPS * piece, width)
        rows = lax.all_gather(sent, PLANE, axis=0, tiled=True)
        weights = mine[:, :, start : start + piece].reshape(plane * GROUPS * piece, local_experts)
        partial = apply_experts(rows, weights, gate, up, down)
        summed = lax.psum_scatter(partial, PLANE, scatter_dimension=0, tiled=True)
        summed = summed.reshape(GROUPS, piece, width)
        results.append(lax.all_to_all(summed, "group", 0, 0, tiled=True))
    result = jnp.concatenate(results, axis=1).reshape(token_total, width)
    return jnp.dot(back, result, preferred_element_type=jnp.float32).astype(jnp.bfloat16)


def local(queries, key_rows, values, sink_logit, out_weight, out_gain, routed_tokens,
          expert_ids, route_weight, routed_gain, expert_gate, expert_up, expert_down):
    experts_out = routed(
        routed_tokens, expert_ids, route_weight, routed_gain, expert_gate, expert_up, expert_down
    )
    mixer_out = attention(queries, key_rows, values, sink_logit, out_weight, out_gain)
    return (mixer_out, experts_out)


def solution(mesh):
    ep, tp = mesh.shape["ep"], mesh.shape["tp"]
    split = Mesh(mesh.devices.reshape(GROUPS, ep // GROUPS, tp), ("group", "member", "tp"))
    every = ("group", "member", "tp")
    placed = (
        P(EP, "tp"),
        P(EP, "tp"),
        P(EP, "tp"),
        P("tp"),
        P("tp", None),
        P(),
        P(every, None),
        P(every, None),
        P(every, None),
        P(),
        P(EP, None, "tp"),
        P(EP, None, "tp"),
        P(EP, None, "tp"),
    )
    return jax.shard_map(
        local,
        mesh=split,
        in_specs=placed,
        out_specs=(P(every, None), P(every, None)),
        check_vma=False,
    )
```

time: 640 us -> 367 us (0.57)
  waiting for transfers between devices: 394 us -> 132 us
  blocking collectives: 0 us -> 87.1 us
  local copies, waits for them, and re-layouts: 89 us -> 14.2 us
  Pallas kernels: 0 us -> 65.8 us
  other arithmetic: 58.9 us -> 9.2 us
  matrix products: 63 us -> 23.1 us
    all_to_all x2 -> x3, waiting for transfers between devices: 232 us -> 26.1 us  [the longest x2 20.5 us: routed(): results.append(lax.all_to_all(summed, 'group', 0, 0, tiled=True))]
    all_to_all x0 -> x3, blocking collectives: none -> 77.3 us  [the longest x2 60 us: routed(): lax.all_to_all(ordered[:, start:start + piece], 'group', 0, 0, tiled=True)]
    pallas_call x0 -> x2, Pallas kernels: none -> 65.8 us  [apply_experts(): pl.pallas_call(expert_kernel, grid=(count // tile,), out_shape=jax.ShapeD...]
    ppermute x2, waiting for transfers between devices: 62 us -> 5.02 us  [the longest x1 4.34 us: padded(): high = lax.ppermute(block[:width], EP, backward)]
    reduce_scatter x1 -> x2, waiting for transfers between devices: 30.2 us -> 75 us  [routed(): summed = lax.psum_scatter(partial, PLANE, scatter_dimension=0, tiled=True)]
    all_gather x3, waiting for transfers between devices: 67.5 us -> 25.8 us  [the longest x2 25.8 us: routed(): rows = lax.all_gather(sent, PLANE, axis=0, tiled=True)]
    dot_general x3 -> x5, matrix products: 50.5 us -> 10.7 us  [the longest x1 3.54 us: attention(): mixed = jnp.dot(attended, full_weight, preferred_element_type=jnp.float32)]
    gather x3 -> x0, local copies, waits for them, and re-layouts: 32 us -> none  [the longest x2 21 us: local(): jnp.take(returned, flat_dest, axis=0).reshape(token_total, TOP, width)]
  transfers between devices with their start and end apart: 8 -> 10, of which waited for: 5 -> 8; matrix products, arithmetic and copies ran while one was open for 22% -> 7% of each run, Pallas kernels for 0% -> 18%
where the time goes in v1:
time: 367 us; the launch traced here: 366 us
  waiting for transfers between devices  132 us (36%)
  blocking collectives  87.1 us (24%)
  Pallas kernels  65.8 us (18%)
  matrix products  23.1 us (6%)
  starting transfers between devices  17.1 us (5%)
  between operations  15.5 us (4%)
  local copies, waits for them, and re-layouts  14.2 us (4%)
  other arithmetic  9.2 us (3%)
    reduce_scatter x2, waiting for transfers between devices, routed(): summed = lax.psum_scatter(partial, PLANE, scatter_dimension=0, tiled=True)  75 us
    pallas_call x2, Pallas kernels, apply_experts(): pl.pallas_call(expert_kernel, grid=(count // tile,), out_shape=jax.ShapeD...  65.8 us
    all_to_all x2, blocking collectives, routed(): lax.all_to_all(ordered[:, start:start + piece], 'group', 0, 0, tiled=True)  60 us
    all_gather x2, waiting for transfers between devices, routed(): rows = lax.all_gather(sent, PLANE, axis=0, tiled=True)  25.8 us
    all_to_all x2, waiting for transfers between devices, routed(): results.append(lax.all_to_all(summed, 'group', 0, 0, tiled=True))  20.5 us
    all_to_all x1, blocking collectives, attention(): lax.all_to_all(attended, 'tp', split_axis=0, concat_axis=1, tiled=True)  17.3 us
    dot_general x2, matrix products, attend_block(): jnp.einsum('hgqk,khd->qhgd', weights, value_block, preferred_element_type...  10 us
    all_gather x1, blocking collectives, routed(): spread = lax.all_gather(spread, PLANE, axis=0, tiled=True)  9.84 us
  transfers between devices with their start and end apart: 10, of which 8 were waited for; matrix products, arithmetic and copies ran while one was open for 7% of the time, Pallas kernels for 18%

profile of v1, /device:TPU:0, one launch (start us, length us, event | category | flops | bytes accessed | tf_op | source)
XLA Modules:
  0.0 365.7 jit_solution(15247870993989550151)
XLA Ops:
  11.1 3.0 convolution_convert_fusion.1
  14.3 32.0 %all_to_all.51 = bf16[4,64,2048]{2,1,0:T(8,128)(2,1)} all-to-all(bf16[4,64,2048]{2,1,0:T(8,128)(2,1)S(1)} %get-tuple-element.110), channel_id=1, replica_groups=mesh['group'=4,'member'=2,'tp'=4] {'group'}, dimensions={0} | all-to-all | bytes 2097152 | tf_op jit(solution)/shard_map/all_to_all | solution.py:166
  46.3 28.1 %all_to_all.52 = bf16[4,64,2048]{2,1,0:T(8,128)(2,1)} all-to-all(bf16[4,64,2048]{2,1,0:T(8,128)(2,1)S(1)} %get-tuple-element.111), channel_id=1, replica_groups=mesh['group'=4,'member'=2,'tp'=4] {'group'}, dimensions={0} | all-to-all | bytes 2097152 | tf_op jit(solution)/shard_map/all_to_all | solution.py:166
  75.7 3.3 all-to-all-start.2
  79.1 5.5 %all-to-all-done.2 = f32[4,1,1024]{2,1,0:T(1,128)S(1)} async-done(((f32[4,1,1024]{2,1,0:T(1,128)}), f32[4,1,1024]{2,1,0:T(1,128)S(1)}, u32[]{:S(2)}, u32[]{:S(2)}) %all-to-all-start.2) | async-done | bytes 16416 | tf_op jit(solution)/shard_map/all_to_all | solution.py:156
  84.6 9.8 %all-gather = f32[32,1,1024]{2,1,0:T(1,128)S(1)} all-gather(f32[4,1,1024]{2,1,0:T(1,128)S(1)} %all-to-all-done.2), channel_id=2, replica_groups=mesh['group'=4,'member'=2,'tp'=4] {'member','tp'}, dimensions={0}, use_global_device_ids=true | all-gather | bytes 147456 | tf_op jit(solution)/shard_map/all_gather | solution.py:157
  94.9 5.4 %all-gather.7.cloned.1.call-done.x_ref = bf16[2048,2048]{1,0:T(8,128)(2,1)} async-done(((bf16[256,2048]{1,0:T(8,128)(2,1)}), bf16[2048,2048]{1,0:T(8,128)(2,1)}) %all-gather.7.cloned.1.call-update) | async-done | bytes 8388624 | tf_op jit(solution)/shard_map/all_gather | solution.py:168
  102.5 32.9 %shard_map.140 = bf16[2048,2048]{1,0:T(8,128)(2,1)} custom-call(bf16[2048,2048]{1,0:T(8,128)(2,1)} %all-gather.7.cloned.1.call-done.x_ref, f32[2048,4]{1,0:T(8,128)S(1)} %bitcast.91, bf16[4,2048,256]{2,1,0:T(8,128)(2,1)S(1)} %copy-done, bf16[4,2048,256]{2,1,0:T(8,128)(2,1)} %up_ref.3, bf16[4,2048,256]{2,1,0:T(8,128)(2,1)} %down_ref.3), custom_call_target="tpu_custom_call" | custom-call | flops 25769803776 | bytes 29360128 | tf_op jit(solution)/shard_map/pallas_call | solution.py:106
  136.1 20.4 %all-gather.9.cloned.1.call-done.x_ref = bf16[2048,2048]{1,0:T(8,128)(2,1)} async-done(((bf16[256,2048]{1,0:T(8,128)(2,1)}), bf16[2048,2048]{1,0:T(8,128)(2,1)}) %all-gather.9.cloned.1.call-update) | async-done | bytes 8388624 | tf_op jit(solution)/shard_map/all_gather | solution.py:168
  158.7 32.9 %shard_map.141 = bf16[2048,2048]{1,0:T(8,128)(2,1)} custom-call(bf16[2048,2048]{1,0:T(8,128)(2,1)} %all-gather.9.cloned.1.call-done.x_ref, f32[2048,4]{1,0:T(8,128)S(1)} %bitcast.92, bf16[4,2048,256]{2,1,0:T(8,128)(2,1)S(1)} %copy-done.1, bf16[4,2048,256]{2,1,0:T(8,128)(2,1)} %up_ref.3, bf16[4,2048,256]{2,1,0:T(8,128)(2,1)} %down_ref.3), custom_call_target="tpu_custom_call" | custom-call | flops 25769803776 | bytes 29360128 | tf_op jit(solution)/shard_map/pallas_call | solution.py:106
  192.7 3.0 collective-permute-start
  197.9 4.3 %collective-permute-done.1 = bf16[128,128]{0,1:T(8,128)(2,1)S(1)} collective-permute-done((bf16[128,128]{0,1:T(8,128)(2,1)S(1)}, bf16[128,128]{0,1:T(8,128)(2,1)S(1)}, u32[]{:S(2)}, u32[]{:S(2)}) %collective-permute-start.1) | collective-permute-done | bytes 32800 | tf_op jit(solution)/shard_map/ppermute | solution.py:30
  202.3 26.4 %while.12 = (s32[]{:T(128)}, bf16[2,512,256]{2,1,0:T(8,128)(2,1)S(1)}, s32[2]{0:T(128)S(1)}, bf16[1280,128]{0,1:T(8,128)(2,1)S(1)}, s32[]{:T(128)}, /*index=5*/b...) while((s32[]{:T(128)}, ...), condition=%wide.region_3.4_spmd, body=%wide.region_0.3_spmd.sunk | while | flops 426778112 | bytes 47478104 | solution.py:74
  205.8 3.2 copy-done.2
  210.6 5.0 %fusion.55 = bf16[64,4,512]{2,0,1:T(8,128)(2,1)S(1)} fusion(f32[4,512]{1,0:T(4,128)S(1)} %exponential_add_fusion.2, f32[4,512]{1,0:T(4,128)S(1)} %broadcast_maximum_fusion.2, f32[768,512,4]{1,0,2:T(8,128)} %copy-done.2, pred[512,768]{0,1:T(8,128)(4,1)S(1)} %fusion.52, bf16[1280,128]{0,1:T(8,128)(2,1)S(1)} %get-tuple-element.202, s32[]{:T(128)S(6)} %select_n.102, ...), kind=kOutput, calls=%fused_computation.10.clone.1 | convolution fusion | flops 210894848 | bytes 7061512 | tf_op jit(solution)/shard_map/while/body/eval_jaxpr/hgqk,khd->qhgd/dot_general | solution.py:69
  223.5 5.0 %fusion.55 = bf16[64,4,512]{2,0,1:T(8,128)(2,1)S(1)} fusion(f32[4,512]{1,0:T(4,128)S(1)} %exponential_add_fusion.2, f32[4,512]{1,0:T(4,128)S(1)} %broadcast_maximum_fusion.2, f32[768,512,4]{1,0,2:T(8,128)} %copy-done.2, pred[512,768]{0,1:T(8,128)(4,1)S(1)} %fusion.52, bf16[1280,128]{0,1:T(8,128)(2,1)S(1)} %get-tuple-element.202, s32[]{:T(128)S(6)} %select_n.102, ...), kind=kOutput, calls=%fused_computation.10.clone.1 | convolution fusion | flops 210894848 | bytes 7061512 | tf_op jit(solution)/shard_map/while/body/eval_jaxpr/hgqk,khd->qhgd/dot_general | solution.py:69
  228.7 17.3 %all_to_all.53 = bf16[4,256,256]{2,1,0:T(8,128)(2,1)S(1)} all-to-all(bf16[4,256,256]{2,1,0:T(8,128)(2,1)S(1)} %bitcast.102), channel_id=1, replica_groups=mesh['group'=4,'member'=2,'tp'=4] {'tp'}, dimensions={0} | all-to-all | bytes 1048576 | tf_op jit(solution)/shard_map/all_to_all | solution.py:76
  245.9 4.8 %reduce-scatter.3.cloned.1.call-done = bf16[256,2048]{1,0:T(8,128)(2,1)} async-done(((bf16[2048,2048]{1,0:T(8,128)(2,1)}), bf16[256,2048]{1,0:T(8,128)(2,1)}) %reduce-scatter.3.cloned.1.call-update) | async-done | bytes 1048592 | tf_op jit(solution)/shard_map/reduce_scatter | solution.py:171
  250.7 4.6 %all-to-all-start.3 = ((bf16[4,64,2048]{2,1,0:T(8,128)(2,1)}), bf16[4,64,2048]{2,1,0:T(8,128)(2,1)S(1)}, u32[]{:S(2)}, u32[]{:S(2)}) async-start(bf16[4,64,2048]{2,1,0:T(8,128)(2,1)} %bitcast.101), calls=%async_computation.4 | async-start | bytes 2097152 | tf_op jit(solution)/shard_map/all_to_all | solution.py:173
  255.3 70.2 %reduce-scatter.5.cloned.1.call-done = bf16[256,2048]{1,0:T(8,128)(2,1)} async-done(((bf16[2048,2048]{1,0:T(8,128)(2,1)}), bf16[256,2048]{1,0:T(8,128)(2,1)}) %reduce-scatter.5.cloned.1.call-update) | async-done | bytes 1048592 | tf_op jit(solution)/shard_map/reduce_scatter | solution.py:171
  325.6 4.6 %all-to-all-start.5 = ((bf16[4,64,2048]{2,1,0:T(8,128)(2,1)}), bf16[4,64,2048]{2,1,0:T(8,128)(2,1)S(1)}, u32[]{:S(2)}, u32[]{:S(2)}) async-start(bf16[4,64,2048]{2,1,0:T(8,128)(2,1)} %bitcast.100), calls=%async_computation.7 | async-start | bytes 2097152 | tf_op jit(solution)/shard_map/all_to_all | solution.py:173
  330.5 3.5 multiply_reduce_fusion
  335.2 20.5 %all-to-all-done.5 = bf16[4,64,2048]{2,1,0:T(8,128)(2,1)S(1)} async-done(((bf16[4,64,2048]{2,1,0:T(8,128)(2,1)}), bf16[4,64,2048]{2,1,0:T(8,128)(2,1)S(1)}, u32[]{:S(2)}, u32[]{:S(2)}) %all-to-all-start.5) | async-done | bytes 1048608 | tf_op jit(solution)/shard_map/all_to_all | solution.py:173
  355.9 2.6 convolution_convert_fusion
  (84 shorter events, 26.6 us)
Async XLA Ops:
  8.0 92.4 %all-gather.7.cloned.1.call-start = ((), (), s32[]{:S(2)}) async-start(), calls=%async_computation.9 | async-start | bytes 9437184 | tf_op jit(solution)/shard_map/all_gather | solution.py:168
  14.3 60.2 %copy-start.7 = (s32[512,2]{0,1:T(2,128)S(1)}, s32[512,2]{0,1:T(2,128)}, u32[]{:S(2)}) copy-start(s32[512,2]{0,1:T(2,128)} %param.22) | copy-start | bytes 12292
  14.3 60.2 %copy-start.9 = (f32[512,2]{0,1:T(2,128)S(1)}, f32[512,2]{0,1:T(2,128)}, u32[]{:S(2)}) copy-start(f32[512,2]{0,1:T(2,128)} %param.23) | copy-start | bytes 12292
  46.3 110.2 %all-gather.9.cloned.1.call-start = ((), (), s32[]{:S(2)}) async-start(), calls=%async_computation.11 | async-start | bytes 9437184 | tf_op jit(solution)/shard_map/all_gather | solution.py:168
  75.7 8.8 %all-to-all-start.2 = ((f32[4,1,1024]{2,1,0:T(1,128)}), f32[4,1,1024]{2,1,0:T(1,128)S(1)}, u32[]{:S(2)}, u32[]{:S(2)}) async-start(f32[4,1,1024]{2,1,0:T(1,128)} %bitcast.24), calls=%async_computation.2 | async-start | bytes 32768 | tf_op jit(solution)/shard_map/all_to_all | solution.py:156
  79.0 171.7 %reduce-scatter.3.cloned.1.call-start = ((), (), s32[]{:S(2)}) async-start(), calls=%async_computation.10 | async-start | bytes 9437184 | tf_op jit(solution)/shard_map/reduce_scatter | solution.py:171
  100.3 2.2 copy-start
  135.5 190.1 %reduce-scatter.5.cloned.1.call-start = ((), (), s32[]{:S(2)}) async-start(), calls=%async_computation.12 | async-start | bytes 9437184 | tf_op jit(solution)/shard_map/reduce_scatter | solution.py:171
  156.5 2.2 copy-start.1
  191.6 0.9 copy-start.4
  191.6 1.0 copy-start.5
  191.6 5.4 %copy-start.3 = (bf16[1024,256]{1,0:T(8,128)(2,1)S(1)}, bf16[1024,256]{1,0:T(8,128)(2,1)}, u32[]{:S(2)}) copy-start(bf16[1024,256]{1,0:T(8,128)(2,1)} %param.15) | copy-start | bytes 1572868
  191.6 10.7 %copy-start.6 = (f32[4]{0:T(128)S(1)}, f32[4]{0:T(128)}, u32[]{:S(2)}) copy-start(f32[4]{0:T(128)} %param.18) | copy-start | bytes 52
  191.6 138.8 %all-gather.5.cloned.1.call-start = ((), (), s32[]{:S(2)}) async-start(), calls=%async_computation.8 | async-start | bytes 5242880 | tf_op jit(solution)/shard_map/all_gather | solution.py:39
  192.7 5.3 %collective-permute-start = (bf16[128,128]{0,1:T(8,128)(2,1)S(1)}, bf16[128,128]{0,1:T(8,128)(2,1)S(1)}, u32[]{:S(2)}, u32[]{:S(2)}) collective-permute-start(bf16[128,128]{0,1:T(8,128)(2,1)S(1)} %get-tuple-element.112), channel_id=1, source_target_pairs={{0,4},{4,8},{8,12},{12,16},{16,20},{20,24},{24,28},{1,5},{5,9},{9,... | collective-permute-start | bytes 98312 | tf_op jit(solution)/shard_map/ppermute | solution.py:29
  195.7 6.6 %collective-permute-start.1 = (bf16[128,128]{0,1:T(8,128)(2,1)S(1)}, bf16[128,128]{0,1:T(8,128)(2,1)S(1)}, u32[]{:S(2)}, u32[]{:S(2)}) collective-permute-start(bf16[128,128]{0,1:T(8,128)(2,1)S(1)} %get-tuple-element.113), channel_id=1, source_target_pairs={{4,0},{8,4},{12,8},{16,12},{20,16},{24,20},{28,24},{5,1},{9,5},{13... | collective-permute-start | bytes 98312 | tf_op jit(solution)/shard_map/ppermute | solution.py:30
  205.7 3.3 copy-start.2
  219.2 2.7 copy-start.2
  250.7 74.8 %all-to-all-start.3 = ((bf16[4,64,2048]{2,1,0:T(8,128)(2,1)}), bf16[4,64,2048]{2,1,0:T(8,128)(2,1)S(1)}, u32[]{:S(2)}, u32[]{:S(2)}) async-start(bf16[4,64,2048]{2,1,0:T(8,128)(2,1)} %bitcast.101), calls=%async_computation.4 | async-start | bytes 2097152 | tf_op jit(solution)/shard_map/all_to_all | solution.py:173
  325.6 30.2 %all-to-all-start.5 = ((bf16[4,64,2048]{2,1,0:T(8,128)(2,1)}), bf16[4,64,2048]{2,1,0:T(8,128)(2,1)S(1)}, u32[]{:S(2)}, u32[]{:S(2)}) async-start(bf16[4,64,2048]{2,1,0:T(8,128)(2,1)} %bitcast.100), calls=%async_computation.7 | async-start | bytes 2097152 | tf_op jit(solution)/shard_map/all_to_all | solution.py:173
  330.2 3.8 %copy-start.8 = (f32[2048]{0:T(1024)S(1)}, f32[2048]{0:T(1024)}, u32[]{:S(2)}) copy-start(f32[2048]{0:T(1024)} %param.20) | copy-start | bytes 24580
Sparse Core Ops, SparseCore 0:
  46.4 53.8 all-gather.6
  102.2 54.2 all-gather.8
  160.0 90.7 reduce-scatter.2
  254.1 71.4 reduce-scatter.4
Sparse Core Ops, SparseCore 1:
  197.1 37.1 all-gather.4
